TPU v7x, 32 devices: a whole 2x2x4 slice. The times are simulated.
32 devices in a mesh: ep: 8 (over z, x), tp: 4 (over y, core).
Axes of the slice: x: 2, y: 2, z: 4, core: 2. Of those that a mesh axis runs over, the one named last changes fastest.
Arguments:
- tokens: bfloat16 [64, 2048], P(('ep', 'tp')), may hold values from -6 to 6
- cache_keys: bfloat16 [64, 1024, 256], P(('ep', 'tp')), may hold values from -360 to 360
- cache_values: bfloat16 [64, 1024, 256], P(('ep', 'tp')), may hold values from -6 to 6
- cache_gates: float32 [64, 2, 1024], P(('ep', 'tp')), may hold values from -256 to 0, as said below
- lengths: int32 [64], P(('ep', 'tp')), may hold values from 1 to 1024, 32768 in all
- routes: int32 [64, 4], P(('ep', 'tp')), may hold values from 0 to 7, all different within a row; in each aligned block of 2 rows (0 to 1, 2 to 3, ...) no two rows name the same one
- route_logits: float32 [64, 4], P(('ep', 'tp')), may hold values from -6 to 6
- attn_gain: float32 [2048], replicated, may hold values from 0.1 to 1.9
- w_query: bfloat16 [2048, 2048], P(None, 'tp'), may hold values from -0.125 to 0.125
- w_keyval: bfloat16 [2048, 512], P(None, 'tp'), may hold values from -0.125 to 0.125
- w_forget: bfloat16 [2048, 2], replicated, may hold values from -0.125 to 0.125
- forget_bias: float32 [2], replicated, may hold values from -1 to 3
- w_out: bfloat16 [2048, 2048], P(None, 'tp'), may hold values from -0.125 to 0.125
- mix_gain: float32 [2048], replicated, may hold values from 0.1 to 1.9
- ffn_gain: float32 [2048], replicated, may hold values from 0.1 to 1.9
- w_gate: bfloat16 [8, 2048, 2048], P('ep', None, 'tp'), may hold values from -0.125 to 0.125
- w_lin: bfloat16 [8, 2048, 2048], P('ep', None, 'tp'), may hold values from -0.125 to 0.125
- gate_bias: float32 [8, 2048], P('ep', 'tp'), may hold values from -12 to 12
- lin_bias: float32 [8, 2048], P('ep', 'tp'), may hold values from -12 to 12
- w_down: bfloat16 [8, 2048, 2048], P('ep', 'tp'), may hold values from -0.125 to 0.125
- post_gain: float32 [2048], replicated, may hold values from 0.1 to 1.9
Outputs:
- updated: bfloat16 [64, 2048], P(('ep', 'tp'))
- new_entries: bfloat16 [64, 512], P(('ep', 'tp'))
Inputs may be any that keep to these rules, and one draw needn't show every extreme that they name: `cache_gates`: along the positions of each sequence and head the values never increase. The lengths of all sequences add up to 32768, and some sequence has exactly 1024. `routes`: each row names 4 different experts; among the rows of one device no expert is named twice; every expert is named by some row.
All inputs are finite; a program needn't handle non-finite values. No bound on the sum of `lengths` on one device may be relied on, other than what follows from the above.
Results may differ from a plain program's by a relative error of at most 0.014.
The roundings to bfloat16 on the way count: a program that leaves them out, or rounds other values in their place, can miss the bound.
Values may be sent and summed in bfloat16 or wider, within the bound.
A program may use at most 64 MiB of HBM per device.

v0:
```python
import functools

import jax
import jax.numpy as jnp
from jax import lax
from jax.experimental import pallas as pl
from jax.experimental.pallas import tpu as pltpu
from jax.sharding import PartitionSpec as P

HEADS = 16
KVH = 2
HDIM = 128


NORM_EPS = 1e-06
SWIGLU_ALPHA = 1.702
SWIGLU_LIMIT = 7.0
NEG_LARGE = -1e30


def rms_scale(values, gain):
    values = values.astype(jnp.float32)
    return values * lax.rsqrt(jnp.mean(values * values, axis=-1, keepdims=True) + NORM_EPS) * gain


def clamped_unit(gate, linear):
    gate = jnp.minimum(gate, SWIGLU_LIMIT)
    linear = jnp.clip(linear, -SWIGLU_LIMIT, SWIGLU_LIMIT)
    return gate * jax.nn.sigmoid(SWIGLU_ALPHA * gate) * (linear + 1.0)


def block_scores(q_four, cache_keys, cache_gates, base, lengths, span, scale):
    seqs = cache_keys.shape[0]
    k_four = cache_keys.reshape(seqs, span, q_four.shape[1], q_four.shape[3])
    scores = (
        jnp.einsum("sgqd,spgd->sgqp", q_four, k_four, preferred_element_type=jnp.float32) * scale
    )
    scores = scores + (base[:, :, None, None] - cache_gates[:, :, None, :])
    place = lax.iota(jnp.int32, span)
    live = place[None, None, None, :] < lengths[:, None, None, None]
    return (jnp.where(live, scores, NEG_LARGE), live)


def per_device(
    tokens,
    cache_keys,
    cache_values,
    cache_gates,
    lengths,
    routes,
    route_logits,
    attn_gain,
    w_query,
    w_keyval,
    w_forget,
    forget_bias,
    w_out,
    mix_gain,
    ffn_gain,
    w_gate,
    w_lin,
    gate_bias,
    lin_bias,
    w_down,
    post_gain,
):
    seqs, width = tokens.shape
    normed = rms_scale(tokens, attn_gain).astype(jnp.bfloat16)
    query_cols = w_query.shape[1]
    pair_cols = w_keyval.shape[1]
    piece = lax.all_gather(normed, "tp", axis=0, tiled=True)
    both = jnp.concatenate(
        [
            jnp.dot(piece, w_query, preferred_element_type=jnp.float32),
            jnp.dot(piece, w_keyval, preferred_element_type=jnp.float32),
        ],
        axis=1,
    )
    gathered = both.astype(jnp.bfloat16)
    owned = lax.all_to_all(gathered, "tp", split_axis=0, concat_axis=1, tiled=True)
    groups = lax.axis_size("tp")
    owned = owned.reshape(seqs, groups, query_cols + pair_cols)
    query = owned[:, :, :query_cols].reshape(seqs, groups * query_cols)
    fresh = owned[:, :, query_cols:].reshape(seqs, groups * pair_cols)
    forget = jax.nn.log_sigmoid(
        jnp.dot(normed, w_forget, preferred_element_type=jnp.float32) + forget_bias
    )
    q_four = query.reshape(seqs, KVH, HEADS // KVH, HDIM)
    new_key = fresh[:, : KVH * HDIM].reshape(seqs, KVH, HDIM)
    new_value = fresh[:, KVH * HDIM :].reshape(seqs, KVH, HDIM)
    span_all = cache_keys.shape[1]
    place = lax.iota(jnp.int32, span_all)
    last = jnp.sum(
        jnp.where(place[None, None, :] == lengths[:, None, None] - 1, cache_gates, 0.0), axis=2
    )
    base = last + forget
    scale = HDIM ** (-0.5)
    own = jnp.einsum("sgqd,sgd->sgq", q_four, new_key, preferred_element_type=jnp.float32) * scale
    values_four = cache_values.reshape(seqs, span_all, KVH, HDIM)
    masked, live = block_scores(q_four, cache_keys, cache_gates, base, lengths, span_all, scale)
    top = jnp.maximum(jnp.max(masked, axis=-1), own)
    expo = jnp.where(live, jnp.exp(masked - top[..., None]), 0.0)
    own_expo = jnp.exp(own - top)
    total = jnp.sum(expo, axis=-1) + own_expo
    weights = (expo / total[..., None]).astype(jnp.bfloat16)
    mixed = jnp.einsum("sgqp,spgd->sgqd", weights, values_four, preferred_element_type=jnp.float32)
    own_weight = (own_expo / total).astype(jnp.bfloat16)
    mixed = (
        mixed
        + own_weight.astype(jnp.float32)[..., None] * new_value.astype(jnp.float32)[:, :, None, :]
    )
    mixed = mixed.reshape(seqs, HEADS * HDIM).astype(jnp.bfloat16)
    projected = jnp.dot(
        lax.all_gather(mixed, "tp", axis=0, tiled=True), w_out, preferred_element_type=jnp.float32
    ).astype(jnp.bfloat16)
    projected = lax.all_to_all(projected, "tp", split_axis=0, concat_axis=1, tiled=True)
    residual = tokens.astype(jnp.float32) + rms_scale(projected, mix_gain)
    expert_in = rms_scale(residual, ffn_gain).astype(jnp.bfloat16)
    experts = lax.axis_size("ep")
    hit = (routes[:, :, None] == lax.iota(jnp.int32, experts)[None, None, :]).astype(jnp.float32)
    probs = jax.nn.softmax(route_logits, axis=-1)
    combine = jnp.sum(probs[:, :, None] * hit, axis=1)
    chosen = jnp.sum(hit, axis=1).T
    outbound = jnp.where(
        chosen[:, :, None] > 0.5, expert_in[None, :, :], jnp.zeros((), jnp.bfloat16)
    )
    slots = outbound.shape[1]
    arrived = lax.all_to_all(outbound, "ep", split_axis=0, concat_axis=0, tiled=True)
    flat = arrived.reshape(experts * slots, width)
    pooled = lax.all_gather(flat, "tp", axis=0, tiled=True)
    piece = pooled
    gate = jnp.dot(piece, w_gate[0], preferred_element_type=jnp.float32) + gate_bias[0]
    linear = jnp.dot(piece, w_lin[0], preferred_element_type=jnp.float32) + lin_bias[0]
    act = clamped_unit(gate, linear).astype(jnp.bfloat16)
    summed = lax.psum_scatter(
        jnp.dot(act, w_down[0], preferred_element_type=jnp.float32).astype(jnp.bfloat16),
        "tp",
        scatter_dimension=0,
        tiled=True,
    )
    returned = lax.all_to_all(
        summed.reshape(experts, slots, width), "ep", split_axis=0, concat_axis=0, tiled=True
    )
    moe = jnp.einsum("se,esd->sd", combine, returned.astype(jnp.float32))
    updated = (residual + rms_scale(moe, post_gain)).astype(jnp.bfloat16)
    return (updated, fresh)


MESH = pl.DeviceIdType.MESH
F32 = jnp.float32
BF16 = jnp.bfloat16


def fused_kernel(
    n_ep,
    n_tp,
    tokens,
    cache_keys,
    cache_values,
    cache_gates,
    lengths,
    routes,
    route_logits,
    attn_gain,
    w_query,
    w_keyval,
    w_forget,
    forget_bias,
    w_out,
    mix_gain,
    ffn_gain,
    w_gate,
    w_lin,
    gate_bias,
    lin_bias,
    w_down,
    post_gain,
    updated,
    fresh,
    v_keys,
    v_values,
    v_gates,
    v_lengths,
    v_logits,
    v_again,
    v_query,
    v_keyval,
    v_forget,
    v_fbias,
    v_out,
    v_mgain,
    v_fgain,
    v_gate,
    v_lin,
    v_gbias,
    v_lbias,
    v_down,
    v_pgain,
    tok_all,
    rt_all,
    qkv_out,
    qkv_all,
    mix_all,
    proj_out,
    proj_all,
    tok_out,
    tok_far,
    disp_out,
    disp_all,
    part_out,
    part_all,
    ret_out,
    ret_all,
    load_sem,
    tok_sem,
    rt_sem,
    qkv_sem,
    mix_sem,
    proj_sem,
    far_sem,
    disp_sem,
    part_sem,
    ret_sem,
):
    my_ep, my_tp = lax.axis_index("ep"), lax.axis_index("tp")
    seqs, width = tokens.shape
    group = n_tp * seqs
    qc, pc = w_query.shape[1], w_keyval.shape[1]

    def tp_peer(d):
        return lax.rem(my_tp + d, n_tp)

    def ep_peer(d):
        return lax.rem(my_ep + d, n_ep)

    def any_peer(d):
        other = lax.rem(my_ep * n_tp + my_tp + d, n_ep * n_tp)
        return other // n_tp, lax.rem(other, n_tp)

    def far_first(n):
        return sorted(range(1, n), key=lambda d: -min(d, n - d))

    tp_far, ep_far, all_far = far_first(n_tp), far_first(n_ep), far_first(n_ep * n_tp)

    names = [
        (tokens, tok_all.at[my_tp]),
        (routes, rt_all.at[my_tp]),
        (attn_gain, v_again),
        (w_query, v_query),
        (w_keyval, v_keyval),
        (w_forget, v_forget),
        (forget_bias, v_fbias),
        (lengths, v_lengths),
        (cache_gates, v_gates),
        (cache_keys, v_keys),
        (cache_values, v_values),
        (w_out, v_out),
        (mix_gain, v_mgain),
        (ffn_gain, v_fgain),
        (w_gate, v_gate),
        (w_lin, v_lin),
        (gate_bias, v_gbias),
        (lin_bias, v_lbias),
        (w_down, v_down),
        (route_logits, v_logits),
        (post_gain, v_pgain),
    ]
    loads = [pltpu.make_async_copy(a, b, load_sem.at[i]) for i, (a, b) in enumerate(names)]
    for load in loads:
        load.start()

    barrier = pltpu.get_barrier_semaphore()
    for d in all_far:
        pl.semaphore_signal(barrier, inc=1, device_id=any_peer(d), device_id_type=MESH)
    loads[0].wait()
    loads[1].wait()
    pl.semaphore_wait(barrier, n_ep * n_tp - 1)

    def tp_copy(d, src, dst, sem):
        return pltpu.make_async_remote_copy(
            src_ref=src,
            dst_ref=dst.at[my_tp],
            send_sem=sem.at[0, d],
            recv_sem=sem.at[1, d],
            device_id=(my_ep, tp_peer(d)),
            device_id_type=MESH,
        )

    def ep_copy(d, src, dst, sem):
        return pltpu.make_async_remote_copy(
            src_ref=src,
            dst_ref=dst.at[my_ep],
            send_sem=sem.at[0, d],
            recv_sem=sem.at[1, d],
            device_id=(ep_peer(d), my_tp),
            device_id_type=MESH,
        )

    def all_copy(d, src, dst, sem):
        peer = any_peer(d)
        return pltpu.make_async_remote_copy(
            src_ref=src.at[peer[0]],
            dst_ref=dst.at[my_ep, my_tp],
            send_sem=sem.at[0, d],
            recv_sem=sem.at[1, d],
            device_id=peer,
            device_id_type=MESH,
        )

    started = []

    def begin(copies):
        for copy in copies:
            copy.start()
        started.extend(copies)
        return copies

    def arrive(copies):
        for copy in copies:
            copy.wait_recv()

    tok_c = begin([tp_copy(d, tok_all.at[my_tp], tok_all, tok_sem) for d in tp_far])
    rt_c = begin([tp_copy(d, rt_all.at[my_tp], rt_all, rt_sem) for d in tp_far])
    for load in loads[2:7]:
        load.wait()
    arrive(tok_c)

    toks = jnp.concatenate([tok_all[s].astype(F32) for s in range(n_tp)], axis=0)
    normed = rms_scale(toks, v_again[...]).astype(BF16)
    q_part = jnp.dot(normed, v_query[...], preferred_element_type=F32)
    kv_part = jnp.dot(normed, v_keyval[...], preferred_element_type=F32)
    both = jnp.concatenate([q_part, kv_part], axis=1).astype(BF16).astype(F32)
    for s in range(n_tp):
        qkv_out[s] = both[s * seqs : (s + 1) * seqs].astype(BF16)
    qkv_c = begin([tp_copy(d, qkv_out.at[tp_peer(d)], qkv_all, qkv_sem) for d in tp_far])
    qkv_all[my_tp] = qkv_out[my_tp]
    arrive(rt_c)
    slots = n_ep * n_tp
    lane = lax.broadcasted_iota(jnp.int32, (group, 128), 1)
    row = lax.broadcasted_iota(jnp.int32, (group, 128), 0)
    named = jnp.zeros((group, 128), F32)
    all_routes = jnp.concatenate([rt_all[s] for s in range(n_tp)], axis=0)
    for c in range(routes.shape[1]):
        named = named + jnp.where(all_routes[:, c : c + 1] == lane // n_tp, 1.0, 0.0)
    named = jnp.where(row // seqs == lane % n_tp, named, 0.0)
    pick = named.T[:slots].astype(BF16)

    picked = jnp.dot(pick, toks.astype(BF16), preferred_element_type=F32)
    for e in range(n_ep):
        tok_out[e] = picked[e * n_tp : (e + 1) * n_tp].astype(BF16)
    far_c = begin([ep_copy(d, tok_out.at[ep_peer(d)], tok_far, far_sem) for d in ep_far])
    tok_far[my_ep] = tok_out[my_ep]

    own_normed = rms_scale(tok_all[my_tp], v_again[...]).astype(BF16)
    raw = lax.dot_general(
        own_normed, v_forget[...], (((1,), (1,)), ((), ())), preferred_element_type=F32
    )
    raw = raw + v_fbias[...]
    forget = jnp.minimum(raw, 0.0) - jnp.log1p(jnp.exp(-jnp.abs(raw)))
    for load in loads[7:11]:
        load.wait()

    span = v_keys.shape[1]
    place = lax.broadcasted_iota(jnp.int32, (1, span), 1)
    heads = HEADS
    per = HEADS // KVH
    first = lax.broadcasted_iota(jnp.int32, (heads, 1), 0) < per
    scale = HDIM ** (-0.5)
    shifts, lives = [], []
    for t in range(seqs):
        length = v_lengths[0:1, t : t + 1]
        gates = v_gates[t]
        last = jnp.sum(jnp.where(place == length - 1, gates, 0.0), axis=1, keepdims=True)
        rows = []
        for g in range(KVH):
            base = last[g : g + 1] + forget[t : t + 1, g : g + 1]
            rows.append(base - gates[g : g + 1])
        shifts.append(jnp.where(first, rows[0], rows[1]))
        lives.append(place < length)

    arrive(qkv_c)
    pieces = [qkv_all[s].astype(F32) for s in range(n_tp)]
    entries = jnp.concatenate([p[:, qc:] for p in pieces], axis=1)
    fresh[...] = entries.astype(BF16)
    mixed_rows = []
    for t in range(seqs):
        q = jnp.concatenate(
            [p[t : t + 1, c * HDIM : (c + 1) * HDIM] for p in pieces for c in range(qc // HDIM)],
            axis=0,
        )
        e = [entries[t : t + 1, c * HDIM : (c + 1) * HDIM] for c in range(2 * KVH)]
        own = jnp.sum(q * jnp.where(first, e[0], e[1]), axis=1, keepdims=True) * scale
        q_wide = jnp.concatenate(
            [jnp.where(first, q, 0.0), jnp.where(first, 0.0, q)], axis=1
        ).astype(BF16)
        scores = lax.dot_general(
            q_wide, v_keys[t], (((1,), (1,)), ((), ())), preferred_element_type=F32
        )
        masked = jnp.where(lives[t], scores * scale + shifts[t], NEG_LARGE)
        top = jnp.maximum(jnp.max(masked, axis=1, keepdims=True), own)
        expo = jnp.where(lives[t], jnp.exp(masked - top), 0.0)
        own_expo = jnp.exp(own - top)
        total = jnp.sum(expo, axis=1, keepdims=True) + own_expo
        weights = (expo / total).astype(BF16)
        wide = jnp.dot(weights, v_values[t], preferred_element_type=F32)
        own_weight = (own_expo / total).astype(BF16).astype(F32)
        mixed = jnp.where(first, wide[:, :HDIM], wide[:, HDIM:])
        mixed = mixed + own_weight * jnp.where(first, e[2], e[3])
        mixed_rows.append(jnp.concatenate([mixed[h : h + 1] for h in range(heads)], axis=1))
    mix_all[my_tp] = jnp.concatenate(mixed_rows, axis=0).astype(BF16)
    mix_c = begin([tp_copy(d, mix_all.at[my_tp], mix_all, mix_sem) for d in tp_far])
    for load in loads[11:14]:
        load.wait()

    arrive(mix_c)
    mixed_all = jnp.concatenate([mix_all[s].astype(F32) for s in range(n_tp)], axis=0).astype(BF16)
    proj = jnp.dot(mixed_all, v_out[...], preferred_element_type=F32).astype(BF16)
    picked = jnp.dot(pick, proj, preferred_element_type=F32)
    for e in range(n_ep):
        disp_out[e] = picked[e * n_tp : (e + 1) * n_tp].astype(BF16)
    disp_c = begin([all_copy(d, disp_out, disp_all, disp_sem) for d in all_far])
    disp_all[my_ep, my_tp] = disp_out[my_ep]
    wide_proj = proj.astype(F32)
    for s in range(n_tp):
        proj_out[s] = wide_proj[s * seqs : (s + 1) * seqs].astype(BF16)
    proj_c = begin([tp_copy(d, proj_out.at[tp_peer(d)], proj_all, proj_sem) for d in tp_far])
    proj_all[my_tp] = proj_out[my_tp]
    arrive(far_c)
    far_toks = jnp.concatenate([tok_far[s].astype(F32) for s in range(n_ep)], axis=0)
    for load in loads[14:]:
        load.wait()
    logits = v_logits[...]
    odds = jnp.exp(logits - jnp.max(logits, axis=1, keepdims=True))
    probs = odds / jnp.sum(odds, axis=1, keepdims=True)
    mine = rt_all[my_tp]
    expert = lax.broadcasted_iota(jnp.int32, (n_ep, 1), 0)
    shares = []
    for t in range(seqs):
        share = jnp.zeros((n_ep, 1), F32)
        for c in range(routes.shape[1]):
            here = expert == mine[t : t + 1, c : c + 1]
            share = share + jnp.where(here, probs[t : t + 1, c : c + 1], 0.0)
        shares.append(share)
    to = lax.broadcasted_iota(jnp.int32, (slots, slots), 0)
    at = lax.broadcasted_iota(jnp.int32, (slots, slots), 1)
    swap = jnp.where((to % n_ep) * n_tp + to // n_ep == at, 1.0, 0.0).astype(BF16)

    arrive(disp_c)
    far_proj = jnp.concatenate(
        [
            jnp.concatenate([disp_all[s, r].astype(F32) for s in range(n_ep)], axis=0)
            for r in range(n_tp)
        ],
        axis=1,
    )
    arrived = far_toks + rms_scale(far_proj, v_mgain[...])
    arrived = rms_scale(arrived, v_fgain[...]).astype(BF16)
    gate = jnp.dot(arrived, v_gate[0], preferred_element_type=F32) + v_gbias[...]
    linear = jnp.dot(arrived, v_lin[0], preferred_element_type=F32) + v_lbias[...]
    act = clamped_unit(gate, linear).astype(BF16)
    act = jnp.dot(swap, act, preferred_element_type=F32).astype(BF16)
    parts = jnp.dot(act, v_down[0], preferred_element_type=F32).astype(BF16)
    for k in range(n_tp):
        part_out[k] = parts[k * n_ep : (k + 1) * n_ep]
    part_c = begin([tp_copy(d, part_out.at[tp_peer(d)], part_all, part_sem) for d in tp_far])
    part_all[my_tp] = part_out[my_tp]
    arrive(proj_c)
    projected = jnp.concatenate([proj_all[s].astype(F32) for s in range(n_tp)], axis=1)
    residual = tok_all[my_tp].astype(F32) + rms_scale(projected, v_mgain[...])
    arrive(part_c)
    summed = part_all[0].astype(F32)
    for k in range(1, n_tp):
        summed = summed + part_all[k].astype(F32)
    summed = summed.astype(BF16).astype(F32)
    for s in range(n_ep):
        ret_out[s] = summed[s : s + 1]
    ret_c = begin([ep_copy(d, ret_out.at[ep_peer(d)], ret_all, ret_sem) for d in ep_far])
    ret_all[my_ep] = ret_out[my_ep]
    arrive(ret_c)
    returned = jnp.concatenate([ret_all[e] for e in range(n_ep)], axis=0)
    moe = jnp.concatenate(
        [jnp.sum(returned * shares[t], axis=0, keepdims=True) for t in range(seqs)], axis=0
    )
    updated[...] = (residual + rms_scale(moe, v_pgain[...])).astype(BF16)
    for copy in started:
        copy.wait_send()


def fused_device(n_ep, n_tp, *args):
    args = [a.reshape(1, -1) if a.ndim == 1 else a for a in args]
    (tokens, keys, values, gates, lengths, routes, logits, again, wq, wkv, wf, fb, wo, mg, fg,
     wg, wl, gb, lb, wd, pg) = args
    args[10] = wf.T
    wf = args[10]
    seqs, width = tokens.shape
    held = [keys, values, gates, lengths, logits, again, wq, wkv, wf, fb, wo, mg, fg, wg, wl, gb,
            lb, wd, pg]
    both = wq.shape[1] + wkv.shape[1]
    vmem = pltpu.VMEM
    dma = pltpu.SemaphoreType.DMA
    scratch = [vmem(a.shape, a.dtype) for a in held] + [
        vmem((n_tp, seqs, width), tokens.dtype),
        vmem((n_tp,) + routes.shape, routes.dtype),
        vmem((n_tp, seqs, both), BF16),
        vmem((n_tp, seqs, both), BF16),
        vmem((n_tp, seqs, HEADS * HDIM), BF16),
        vmem((n_tp, seqs, wo.shape[1]), BF16),
        vmem((n_tp, seqs, wo.shape[1]), BF16),
        vmem((n_ep, n_tp, width), BF16),
        vmem((n_ep, n_tp, width), BF16),
        vmem((n_ep, n_tp, wo.shape[1]), BF16),
        vmem((n_ep, n_tp, n_tp, wo.shape[1]), BF16),
        vmem((n_tp, n_ep, width), BF16),
        vmem((n_tp, n_ep, width), BF16),
        vmem((n_ep, 1, width), F32),
        vmem((n_ep, 1, width), F32),
        dma((len(args),)),
        dma((2, n_tp)),
        dma((2, n_tp)),
        dma((2, n_tp)),
        dma((2, n_tp)),
        dma((2, n_tp)),
        dma((2, n_ep)),
        dma((2, n_ep * n_tp)),
        dma((2, n_tp)),
        dma((2, n_ep)),
    ]
    return pl.pallas_call(
        functools.partial(fused_kernel, n_ep, n_tp),
        out_shape=(
            jax.ShapeDtypeStruct((seqs, width), BF16),
            jax.ShapeDtypeStruct((seqs, n_tp * wkv.shape[1]), BF16),
        ),
        in_specs=[pl.BlockSpec(memory_space=pl.ANY)] * len(args),
        out_specs=(pl.BlockSpec(memory_space=vmem), pl.BlockSpec(memory_space=vmem)),
        scratch_shapes=scratch,
        compiler_params=pltpu.CompilerParams(
            collective_id=0, has_side_effects=True, vmem_limit_bytes=66_000_000
        ),
        name="decode_layer",
    )(*args)


def hand_over(updated, fresh, updated_out, fresh_out):
    updated_out[...] = updated[...]
    fresh_out[...] = fresh[...]


def plain_copy(results):
    vmem = pl.BlockSpec(memory_space=pltpu.VMEM)
    return pl.pallas_call(
        hand_over,
        out_shape=tuple(jax.ShapeDtypeStruct(r.shape, r.dtype) for r in results),
        in_specs=[vmem, vmem],
        out_specs=(vmem, vmem),
        name="hand_over",
    )(*results)


def fits(args, n_ep, n_tp):
    tokens, routes, wq, wkv = args[0], args[5], args[8], args[9]
    return (
        wq.shape[1] % HDIM == 0
        and wkv.shape[1] % HDIM == 0
        and n_ep * n_tp <= 128
        and n_ep % 8 == 0
        and (n_tp * tokens.shape[0]) % 8 == 0
        and KVH == 2
    )


def solution(mesh):
    in_specs = (
        P(("ep", "tp"), None),
        P(("ep", "tp"), None, None),
        P(("ep", "tp"), None, None),
        P(("ep", "tp"), None, None),
        P(("ep", "tp")),
        P(("ep", "tp"), None),
        P(("ep", "tp"), None),
        P(),
        P(None, "tp"),
        P(None, "tp"),
        P(),
        P(),
        P(None, "tp"),
        P(),
        P(),
        P("ep", None, "tp"),
        P("ep", None, "tp"),
        P("ep", "tp"),
        P("ep", "tp"),
        P("ep", "tp", None),
        P(),
    )
    out_specs = (P(("ep", "tp"), None), P(("ep", "tp"), None))
    n_ep, n_tp = mesh.shape["ep"], mesh.shape["tp"]

    def body(*args):
        if fits(args, n_ep, n_tp):
            return plain_copy(fused_device(n_ep, n_tp, *args))
        return per_device(*args)

    return jax.shard_map(
        body, mesh=mesh, in_specs=in_specs, out_specs=out_specs, check_vma=False
    )
```

profile of v0, /device:TPU:0, one launch (start us, length us, event | category | flops | bytes accessed | tf_op | source)
XLA Modules:
  0.0 36.3 jit_solution(6205101356705635531)
XLA Ops:
  0.6 34.4 %decode_layer.1 = (bf16[2,2048]{1,0:T(2,128)(2,1)}, bf16[2,512]{1,0:T(2,128)(2,1)}) custom-call(bf16[2,2048]{1,0:T(2,128)(2,1)} %tokens.1, bf16[2,1024,256]{2,1,0:T(8,128)(2,1)} %cache_keys.1, bf16[2,1024,256]{2,1,0:T(8,128)(2,1)} %cache_values.1, f32[2,2,1024]{2,1,0:T(2,128)} %cache_gates.1, s32[1,2]{1,0:T(1,128)} %bitcast.12, s32[2,4]{1,0:T(2,128)} %routes.1, ...), custom_call_target="tpu_custom_call" | custom-call | tf_op jit(solution)/shard_map/decode_layer/pallas_call | solution.py:528
  35.0 1.3 %hand_over.1 = (bf16[2,2048]{1,0:T(2,128)(2,1)}, bf16[2,512]{1,0:T(2,128)(2,1)}) custom-call(bf16[2,2048]{1,0:T(2,128)(2,1)} %get-tuple-element.4.updated, bf16[2,512]{1,0:T(2,128)(2,1)} %get-tuple-element.5.fresh), custom_call_target="tpu_custom_call" | custom-call | tf_op jit(solution)/shard_map/hand_over/pallas_call | solution.py:551
where the time goes:
time: 36.6 us; the launch traced here: 36.3 us
  Pallas kernels  35.7 us (98%)
  between operations  0.65 us (2%)
    pallas_call x1, Pallas kernels, fused_device(): pl.pallas_call(functools.partial(fused_kernel, n_ep, n_tp), out_shape=(ja...  34.4 us
    pallas_call x1, Pallas kernels, plain_copy(): pl.pallas_call(hand_over, out_shape=tuple((jax.ShapeDtypeStruct(r.shape,...  1.3 us

commit v1 on v0

v1 whole, which is shorter than its diff:
```python
import functools

import jax
import jax.numpy as jnp
from jax import lax
from jax.experimental import pallas as pl
from jax.experimental.pallas import tpu as pltpu
from jax.sharding import PartitionSpec as P

HEADS = 16
KVH = 2
HDIM = 128


NORM_EPS = 1e-06
SWIGLU_ALPHA = 1.702
SWIGLU_LIMIT = 7.0
NEG_LARGE = -1e30


def rms_scale(values, gain):
    values = values.astype(jnp.float32)
    return values * lax.rsqrt(jnp.mean(values * values, axis=-1, keepdims=True) + NORM_EPS) * gain


def clamped_unit(gate, linear):
    gate = jnp.minimum(gate, SWIGLU_LIMIT)
    linear = jnp.clip(linear, -SWIGLU_LIMIT, SWIGLU_LIMIT)
    return gate * jax.nn.sigmoid(SWIGLU_ALPHA * gate) * (linear + 1.0)


def block_scores(q_four, cache_keys, cache_gates, base, lengths, span, scale):
    seqs = cache_keys.shape[0]
    k_four = cache_keys.reshape(seqs, span, q_four.shape[1], q_four.shape[3])
    scores = (
        jnp.einsum("sgqd,spgd->sgqp", q_four, k_four, preferred_element_type=jnp.float32) * scale
    )
    scores = scores + (base[:, :, None, None] - cache_gates[:, :, None, :])
    place = lax.iota(jnp.int32, span)
    live = place[None, None, None, :] < lengths[:, None, None, None]
    return (jnp.where(live, scores, NEG_LARGE), live)


def per_device(
    tokens,
    cache_keys,
    cache_values,
    cache_gates,
    lengths,
    routes,
    route_logits,
    attn_gain,
    w_query,
    w_keyval,
    w_forget,
    forget_bias,
    w_out,
    mix_gain,
    ffn_gain,
    w_gate,
    w_lin,
    gate_bias,
    lin_bias,
    w_down,
    post_gain,
):
    seqs, width = tokens.shape
    normed = rms_scale(tokens, attn_gain).astype(jnp.bfloat16)
    query_cols = w_query.shape[1]
    pair_cols = w_keyval.shape[1]
    piece = lax.all_gather(normed, "tp", axis=0, tiled=True)
    both = jnp.concatenate(
        [
            jnp.dot(piece, w_query, preferred_element_type=jnp.float32),
            jnp.dot(piece, w_keyval, preferred_element_type=jnp.float32),
        ],
        axis=1,
    )
    gathered = both.astype(jnp.bfloat16)
    owned = lax.all_to_all(gathered, "tp", split_axis=0, concat_axis=1, tiled=True)
    groups = lax.axis_size("tp")
    owned = owned.reshape(seqs, groups, query_cols + pair_cols)
    query = owned[:, :, :query_cols].reshape(seqs, groups * query_cols)
    fresh = owned[:, :, query_cols:].reshape(seqs, groups * pair_cols)
    forget = jax.nn.log_sigmoid(
        jnp.dot(normed, w_forget, preferred_element_type=jnp.float32) + forget_bias
    )
    q_four = query.reshape(seqs, KVH, HEADS // KVH, HDIM)
    new_key = fresh[:, : KVH * HDIM].reshape(seqs, KVH, HDIM)
    new_value = fresh[:, KVH * HDIM :].reshape(seqs, KVH, HDIM)
    span_all = cache_keys.shape[1]
    place = lax.iota(jnp.int32, span_all)
    last = jnp.sum(
        jnp.where(place[None, None, :] == lengths[:, None, None] - 1, cache_gates, 0.0), axis=2
    )
    base = last + forget
    scale = HDIM ** (-0.5)
    own = jnp.einsum("sgqd,sgd->sgq", q_four, new_key, preferred_element_type=jnp.float32) * scale
    values_four = cache_values.reshape(seqs, span_all, KVH, HDIM)
    masked, live = block_scores(q_four, cache_keys, cache_gates, base, lengths, span_all, scale)
    top = jnp.maximum(jnp.max(masked, axis=-1), own)
    expo = jnp.where(live, jnp.exp(masked - top[..., None]), 0.0)
    own_expo = jnp.exp(own - top)
    total = jnp.sum(expo, axis=-1) + own_expo
    weights = (expo / total[..., None]).astype(jnp.bfloat16)
    mixed = jnp.einsum("sgqp,spgd->sgqd", weights, values_four, preferred_element_type=jnp.float32)
    own_weight = (own_expo / total).astype(jnp.bfloat16)
    mixed = (
        mixed
        + own_weight.astype(jnp.float32)[..., None] * new_value.astype(jnp.float32)[:, :, None, :]
    )
    mixed = mixed.reshape(seqs, HEADS * HDIM).astype(jnp.bfloat16)
    projected = jnp.dot(
        lax.all_gather(mixed, "tp", axis=0, tiled=True), w_out, preferred_element_type=jnp.float32
    ).astype(jnp.bfloat16)
    projected = lax.all_to_all(projected, "tp", split_axis=0, concat_axis=1, tiled=True)
    residual = tokens.astype(jnp.float32) + rms_scale(projected, mix_gain)
    expert_in = rms_scale(residual, ffn_gain).astype(jnp.bfloat16)
    experts = lax.axis_size("ep")
    hit = (routes[:, :, None] == lax.iota(jnp.int32, experts)[None, None, :]).astype(jnp.float32)
    probs = jax.nn.softmax(route_logits, axis=-1)
    combine = jnp.sum(probs[:, :, None] * hit, axis=1)
    chosen = jnp.sum(hit, axis=1).T
    outbound = jnp.where(
        chosen[:, :, None] > 0.5, expert_in[None, :, :], jnp.zeros((), jnp.bfloat16)
    )
    slots = outbound.shape[1]
    arrived = lax.all_to_all(outbound, "ep", split_axis=0, concat_axis=0, tiled=True)
    flat = arrived.reshape(experts * slots, width)
    pooled = lax.all_gather(flat, "tp", axis=0, tiled=True)
    piece = pooled
    gate = jnp.dot(piece, w_gate[0], preferred_element_type=jnp.float32) + gate_bias[0]
    linear = jnp.dot(piece, w_lin[0], preferred_element_type=jnp.float32) + lin_bias[0]
    act = clamped_unit(gate, linear).astype(jnp.bfloat16)
    summed = lax.psum_scatter(
        jnp.dot(act, w_down[0], preferred_element_type=jnp.float32).astype(jnp.bfloat16),
        "tp",
        scatter_dimension=0,
        tiled=True,
    )
    returned = lax.all_to_all(
        summed.reshape(experts, slots, width), "ep", split_axis=0, concat_axis=0, tiled=True
    )
    moe = jnp.einsum("se,esd->sd", combine, returned.astype(jnp.float32))
    updated = (residual + rms_scale(moe, post_gain)).astype(jnp.bfloat16)
    return (updated, fresh)


MESH = pl.DeviceIdType.MESH
F32 = jnp.float32
BF16 = jnp.bfloat16


def flip(value, mask, size):
    out, bit = value, 1
    while bit < size:
        if mask & bit:
            out = out + bit - 2 * bit * lax.rem(value // bit, 2)
        bit *= 2
    return out


def wait_bytes(ref, sem):
    pltpu.make_async_copy(ref, ref, sem).wait()


def block_rms(block, width):
    squares = jnp.sum(block * block, axis=1, keepdims=True)
    return lax.rsqrt(jnp.sum(squares, axis=0, keepdims=True) * (1.0 / width) + NORM_EPS)


def fused_kernel(
    n_ep,
    n_tp,
    tokens,
    cache_keys,
    cache_values,
    cache_gates,
    lengths,
    routes,
    route_logits,
    attn_gain,
    w_query,
    w_keyval,
    w_forget,
    forget_bias,
    w_out,
    mix_gain,
    mix_gain_l,
    ffn_gain,
    w_gate,
    w_lin,
    gate_bias,
    lin_bias,
    w_down,
    post_gain_l,
    updated,
    fresh,
    v_kv,
    v_gates,
    v_lengths,
    v_logits,
    v_again,
    v_qkv,
    v_forget,
    v_fbias,
    v_out,
    v_mgain,
    v_mgain_l,
    v_fgain,
    v_gl,
    v_gbias,
    v_lbias,
    v_down,
    v_pgain_l,
    tok_all,
    rt_all,
    qkv_out,
    qkv_all,
    mix_all,
    proj_out,
    proj_all,
    tok_out,
    tok_far,
    disp_out,
    disp_all,
    part_out,
    part_all,
    s_tok,
    s_qkv,
    s_mix,
    s_proj,
    s_far,
    s_disp,
    s_part,
    s_tok_l,
    s_proj_l,
    s_share,
    load_sem,
    tok_sem,
    rt_sem,
    qkv_sem,
    mix_sem,
    proj_sem,
    far_sem,
    disp_sem,
    part_sem,
    near_sem,
):
    my_ep, my_tp = lax.axis_index("ep"), lax.axis_index("tp")
    seqs, width = tokens.shape
    group = n_tp * seqs
    slots = n_ep * n_tp
    qc = w_query.shape[1]
    oc = w_out.shape[1]
    ff = w_down.shape[1]
    blocks = width // 128
    q_sub = qc // HDIM
    heads = HEADS
    per = HEADS // KVH
    scale = HDIM ** (-0.5)

    ep_at = [flip(my_ep, k, n_ep) for k in range(n_ep)]
    tp_at = [flip(my_tp, k, n_tp) for k in range(n_tp)]
    me = my_ep * n_tp + my_tp

    def tell(sem, ep, tp):
        pl.semaphore_signal(sem, inc=1, device_id=(ep, tp), device_id_type=MESH)

    def tell_near(sem):
        tell(sem, ep_at[1], my_tp)

        @pl.when(my_ep >= 2)
        def _():
            tell(sem, my_ep - 2, my_tp)

        @pl.when(my_ep + 2 < n_ep)
        def _():
            tell(sem, my_ep + 2, my_tp)

    near = 1 + jnp.minimum(my_ep // 2, 1) + jnp.minimum((n_ep - 1 - my_ep) // 2, 1)

    def heard(k):
        pl.semaphore_wait(near_sem.at[k], near)

    load_list, waits = [], {}

    def load(key, *pairs, whole=None):
        k = len(waits)
        load_list.extend((a, b, k) for a, b in pairs)
        waits[key] = (pairs[0][1] if whole is None else whole, k)

    def loaded(*keys):
        for key in keys:
            ref, k = waits[key]
            wait_bytes(ref, load_sem.at[k])

    load("tok", (tokens, tok_all.at[0]))
    load("rt", (routes, rt_all.at[0]))
    load("again", (attn_gain, v_again))
    load("qkv", (w_query, v_qkv.at[:, :qc]), (w_keyval, v_qkv.at[:, qc:]), whole=v_qkv)
    load("forget", (w_forget, v_forget))
    load("fbias", (forget_bias, v_fbias))
    load("lengths", (lengths, v_lengths))
    load("gates", (cache_gates, v_gates))
    load("kv", (cache_keys, v_kv.at[0]), (cache_values, v_kv.at[1]), whole=v_kv)
    load("out", (w_out, v_out))
    load("mgain", (mix_gain, v_mgain))
    load("mgain_l", (mix_gain_l, v_mgain_l))
    load("fgain", (ffn_gain, v_fgain))
    load("gl", (w_gate.at[0], v_gl.at[:, :ff]), (w_lin.at[0], v_gl.at[:, ff:]), whole=v_gl)
    load("gbias", (gate_bias, v_gbias))
    load("lbias", (lin_bias, v_lbias))
    load("down", (w_down.at[0], v_down))
    load("logits", (route_logits, v_logits))
    load("pgain_l", (post_gain_l, v_pgain_l))

    barrier = pltpu.get_barrier_semaphore()
    for j in range(n_tp - 1, 0, -1):
        tell(barrier, my_ep, tp_at[j])
    copies = [pltpu.make_async_copy(a, b, load_sem.at[k]) for a, b, k in load_list]
    copies[0].start()
    tell_near(barrier)
    for copy in copies[1:]:
        copy.start()

    def tp_send(src, dst, sem):
        for j in range(n_tp - 1, 0, -1):
            pltpu.make_async_remote_copy(
                src_ref=src(tp_at[j]),
                dst_ref=dst.at[j],
                send_sem=sem.at[0],
                recv_sem=sem.at[1],
                device_id=(my_ep, tp_at[j]),
                device_id_type=MESH,
            ).start()

    sent = []

    def arrive(ref, sem):
        wait_bytes(ref.at[pl.ds(1, ref.shape[0] - 1)], sem.at[1])
        sent.append((ref, sem))

    loaded("tok", "rt")
    pl.semaphore_wait(barrier, n_tp - 1 + near)
    tp_send(lambda p: tok_all.at[0], tok_all, tok_sem)
    tp_send(lambda p: rt_all.at[0], rt_all, rt_sem)
    tell_near(near_sem.at[0])
    s_qkv[...] = jnp.zeros_like(s_qkv)
    loaded("again", "qkv")
    arrive(tok_all, tok_sem)

    for s in range(n_tp):
        piece = tok_all[tp_at[s]].astype(F32)
        for b in range(blocks):
            s_tok[b, s * seqs : (s + 1) * seqs, :] = piece[:, b * 128 : (b + 1) * 128]
    toks = jnp.concatenate([s_tok[b] for b in range(blocks)], axis=1)
    normed = rms_scale(toks, v_again[...]).astype(BF16)
    both = jnp.dot(normed, v_qkv[...], preferred_element_type=F32)
    for c in range(q_sub + 1):
        s_qkv[pl.ds(c, group, stride=8), :] = both[:, c * HDIM : (c + 1) * HDIM]
    for s in range(n_tp):
        qkv_out[s] = s_qkv[s * seqs * 8 : (s + 1) * seqs * 8, :].astype(BF16)
    tp_send(lambda p: qkv_out.at[p], qkv_all, qkv_sem)
    heard(0)
    tell_near(near_sem.at[1])
    qkv_all[0] = qkv_out[my_tp]

    loaded("forget", "fbias", "lengths", "gates")
    own_normed = rms_scale(tok_all[0], v_again[...]).astype(BF16)
    raw = lax.dot_general(
        own_normed, v_forget[...], (((1,), (1,)), ((), ())), preferred_element_type=F32
    )
    raw = raw + v_fbias[...]
    forget = jnp.minimum(raw, 0.0) - jnp.log1p(jnp.exp(-jnp.abs(raw)))
    span = cache_keys.shape[1]
    place = lax.broadcasted_iota(jnp.int32, (1, span), 1)
    first = lax.broadcasted_iota(jnp.int32, (heads, 1), 0) < per
    shifts, lives = [], []
    for t in range(seqs):
        length = v_lengths[0:1, t : t + 1]
        gates = v_gates[t]
        last = jnp.sum(jnp.where(place == length - 1, gates, 0.0), axis=1, keepdims=True)
        rows = []
        for g in range(KVH):
            base = last[g : g + 1] + forget[t : t + 1, g : g + 1]
            rows.append(base - gates[g : g + 1])
        shifts.append(jnp.where(first, rows[0], rows[1]))
        lives.append(place < length)
    heard(1)
    tell_near(near_sem.at[2])
    loaded("kv")
    arrive(qkv_all, qkv_sem)

    pieces = [qkv_all[tp_at[s]].astype(F32) for s in range(n_tp)]
    entries = []
    for t in range(seqs):
        q = jnp.concatenate([p[t * 8 : t * 8 + q_sub] for p in pieces], axis=0)
        e = [p[t * 8 + q_sub : t * 8 + q_sub + 1] for p in pieces]
        entries.append(jnp.concatenate(e, axis=1))
        own = jnp.sum(q * jnp.where(first, e[0], e[1]), axis=1, keepdims=True) * scale
        q_wide = jnp.concatenate(
            [jnp.where(first, q, 0.0), jnp.where(first, 0.0, q)], axis=1
        ).astype(BF16)
        scores = lax.dot_general(
            q_wide, v_kv[0, t], (((1,), (1,)), ((), ())), preferred_element_type=F32
        )
        masked = jnp.where(lives[t], scores * scale + shifts[t], NEG_LARGE)
        top = jnp.maximum(jnp.max(masked, axis=1, keepdims=True), own)
        expo = jnp.exp(masked - top)
        own_expo = jnp.exp(own - top)
        total = jnp.sum(expo, axis=1, keepdims=True) + own_expo
        wide = jnp.dot(expo.astype(BF16), v_kv[1, t], preferred_element_type=F32)
        mixed = jnp.where(first, wide[:, :HDIM], wide[:, HDIM:])
        mixed = (mixed + own_expo * jnp.where(first, e[2], e[3])) / total
        mix_all[0, t * heads : (t + 1) * heads, :] = mixed.astype(BF16)
    tp_send(lambda p: mix_all.at[0], mix_all, mix_sem)
    fresh[...] = jnp.concatenate(entries, axis=0).astype(BF16)

    arrive(rt_all, rt_sem)
    named = []
    for c in range(seqs):
        rows = jnp.concatenate([rt_all[tp_at[s]][c : c + 1] for s in range(n_tp)], axis=0)
        picks = [
            jnp.broadcast_to(rows[:, k : k + 1], (n_tp, 128)) for k in range(routes.shape[1])
        ]
        named.append(picks)

    def chosen(c, e):
        hit = named[c][0] == e
        for k in range(1, routes.shape[1]):
            hit = jnp.logical_or(hit, named[c][k] == e)
        return hit

    masks = [[chosen(c, e) for e in range(n_ep)] for c in range(1, seqs)]

    def choose(scratch, columns, out):
        for b in range(columns // 128):
            lanes = slice(b * 128, (b + 1) * 128)
            rows = [scratch[b, pl.ds(c, n_tp, stride=seqs), :] for c in range(seqs)]
            for e in range(n_ep):
                row = rows[0]
                for c in range(1, seqs):
                    row = jnp.where(masks[c - 1][e], rows[c], row)
                out[e, :, lanes] = row.astype(BF16)

    choose(s_tok, width, tok_out)
    heard(2)
    tell_near(near_sem.at[3])
    for i in range(n_ep - 1, 0, -1):
        pltpu.make_async_remote_copy(
            src_ref=tok_out.at[ep_at[i]],
            dst_ref=tok_far.at[i],
            send_sem=far_sem.at[0],
            recv_sem=far_sem.at[1],
            device_id=(ep_at[i], my_tp),
            device_id_type=MESH,
        ).start()
    tok_far[0] = tok_out[my_ep]

    for b in range(blocks):
        s_tok_l[pl.ds(b, seqs, stride=blocks), :] = tok_all[0, :, b * 128 : (b + 1) * 128].astype(
            F32
        )
    loaded("out", "mgain", "mgain_l", "fgain", "gl", "gbias", "lbias", "down", "logits", "pgain_l")
    logits = v_logits[...]
    odds = jnp.exp(logits - jnp.max(logits, axis=1, keepdims=True))
    probs = odds / jnp.sum(odds, axis=1, keepdims=True)
    mine = rt_all[0]
    for t in range(seqs):
        at = [jnp.broadcast_to(mine[t : t + 1, c : c + 1], (8, 128)) for c in range(mine.shape[1])]
        of = [jnp.broadcast_to(probs[t : t + 1, c : c + 1], (8, 128)) for c in range(len(at))]
        for e in range(n_ep):
            share = jnp.where(at[0] == e, of[0], 0.0)
            for c in range(1, len(at)):
                share = share + jnp.where(at[c] == e, of[c], 0.0)
            s_share[t, e] = share
    heard(3)
    arrive(mix_all, mix_sem)

    for s in range(n_tp):
        size = seqs * heads
        s_mix[s * size : (s + 1) * size, :] = mix_all[tp_at[s]].astype(F32)
    mixed_all = jnp.concatenate(
        [s_mix[pl.ds(h, group, stride=heads), :] for h in range(heads)], axis=1
    ).astype(BF16)
    proj = jnp.dot(mixed_all, v_out[...], preferred_element_type=F32)
    for b in range(oc // 128):
        s_proj[b] = proj[:, b * 128 : (b + 1) * 128]
    choose(s_proj, oc, disp_out)

    def all_send(src, dst, sem):
        for i in range(n_ep - 1, -1, -1):
            for j in range(n_tp - 1, -1, -1):
                if i or j:
                    pltpu.make_async_remote_copy(
                        src_ref=src(ep_at[i], tp_at[j]),
                        dst_ref=dst.at[i * n_tp + j],
                        send_sem=sem.at[0],
                        recv_sem=sem.at[1],
                        device_id=(ep_at[i], tp_at[j]),
                        device_id_type=MESH,
                    ).start()

    all_send(lambda ep, tp: disp_out.at[ep], disp_all, disp_sem)
    disp_all[0] = disp_out[my_ep]
    for s in range(n_tp):
        proj_out[s] = proj[s * seqs : (s + 1) * seqs].astype(BF16)
    tp_send(lambda p: proj_out.at[p], proj_all, proj_sem)
    proj_all[0] = proj_out[my_tp]
    arrive(tok_far, far_sem)
    for e in range(n_ep):
        s_far[e * n_tp : (e + 1) * n_tp, :] = tok_far[ep_at[e]].astype(F32)

    arrive(disp_all, disp_sem)
    for e in range(n_ep):
        for r in range(n_tp):
            s_disp[e * n_tp : (e + 1) * n_tp, r * oc : (r + 1) * oc] = disp_all[
                ep_at[e] * n_tp + tp_at[r]
            ].astype(F32)
    arrived = s_far[...] + rms_scale(s_disp[...], v_mgain[...])
    power = lax.rsqrt(jnp.mean(arrived * arrived, axis=1, keepdims=True) + NORM_EPS)
    expert_in = (arrived * v_fgain[...]).astype(BF16)
    hidden = jnp.dot(expert_in, v_gl[...], preferred_element_type=F32) * power
    act = clamped_unit(hidden[:, :ff] + v_gbias[...], hidden[:, ff:] + v_lbias[...]).astype(BF16)
    parts = jnp.dot(act, v_down[...], preferred_element_type=F32)
    for b in range(blocks):
        s_part[pl.ds(b, slots, stride=blocks), :] = parts[:, b * 128 : (b + 1) * 128]
    for s in range(slots):
        part_out[s] = s_part[s * blocks : (s + 1) * blocks, :].astype(BF16)
    all_send(lambda ep, tp: part_out.at[ep * n_tp + tp], part_all, part_sem)
    part_all[0] = part_out[me]

    arrive(proj_all, proj_sem)
    for s in range(n_tp):
        piece = proj_all[tp_at[s]].astype(F32)
        for b in range(oc // 128):
            s_proj_l[pl.ds(s * (oc // 128) + b, seqs, stride=blocks), :] = piece[
                :, b * 128 : (b + 1) * 128
            ]
    residual = []
    for t in range(seqs):
        rows = slice(t * blocks, (t + 1) * blocks)
        own_proj = s_proj_l[rows, :]
        residual.append(s_tok_l[rows, :] + own_proj * block_rms(own_proj, width) * v_mgain_l[...])

    arrive(part_all, part_sem)
    moe = [jnp.zeros((blocks, 128), F32) for _ in range(seqs)]
    for e in range(n_ep):
        summed = part_all[ep_at[e] * n_tp + tp_at[0]].astype(F32)
        for r in range(1, n_tp):
            summed = summed + part_all[ep_at[e] * n_tp + tp_at[r]].astype(F32)
        summed = summed.astype(BF16).astype(F32)
        for t in range(seqs):
            share = jnp.concatenate([s_share[t, e]] * (blocks // 8), axis=0)
            moe[t] = moe[t] + summed * share
    for t in range(seqs):
        rows = slice(t * blocks, (t + 1) * blocks)
        updated[rows, :] = residual[t] + moe[t] * block_rms(moe[t], width) * v_pgain_l[...]
    for ref, sem in sent:
        wait_bytes(ref.at[pl.ds(1, ref.shape[0] - 1)], sem.at[0])


def fused_device(n_ep, n_tp, *args):
    args = [a.reshape(1, -1) if a.ndim == 1 else a for a in args]
    (tokens, keys, values, gates, lengths, routes, logits, again, wq, wkv, wf, fb, wo, mg, fg,
     wg, wl, gb, lb, wd, pg) = args
    seqs, width = tokens.shape
    blocks = width // 128
    mg_l, pg_l, wf = mg.reshape(blocks, 128), pg.reshape(blocks, 128), wf.T
    both = wq.shape[1] + wkv.shape[1]
    ff, oc = wd.shape[1], wo.shape[1]
    slots, group = n_ep * n_tp, n_tp * seqs
    vmem = pltpu.VMEM
    dma = pltpu.SemaphoreType.DMA

    def like(a):
        return vmem(a.shape, a.dtype)

    operands = [tokens, keys, values, gates, lengths, routes, logits, again, wq, wkv, wf, fb, wo,
                mg, mg_l, fg, wg, wl, gb, lb, wd, pg_l]
    scratch = [
        vmem((2,) + keys.shape, keys.dtype),
        like(gates),
        like(lengths),
        like(logits),
        like(again),
        vmem((width, both), wq.dtype),
        like(wf),
        like(fb),
        like(wo),
        like(mg),
        like(mg_l),
        like(fg),
        vmem((width, 2 * ff), wg.dtype),
        like(gb),
        like(lb),
        vmem(wd.shape[1:], wd.dtype),
        like(pg_l),
        vmem((n_tp, seqs, width), tokens.dtype),
        vmem((n_tp,) + routes.shape, routes.dtype),
        vmem((n_tp, seqs * 8, HDIM), BF16),
        vmem((n_tp, seqs * 8, HDIM), BF16),
        vmem((n_tp, seqs * HEADS, HDIM), BF16),
        vmem((n_tp, seqs, oc), BF16),
        vmem((n_tp, seqs, oc), BF16),
        vmem((n_ep, n_tp, width), BF16),
        vmem((n_ep, n_tp, width), BF16),
        vmem((n_ep, n_tp, oc), BF16),
        vmem((slots, n_tp, oc), BF16),
        vmem((slots, blocks, 128), BF16),
        vmem((slots, blocks, 128), BF16),
        vmem((blocks, group, 128), F32),
        vmem((group * 8, HDIM), F32),
        vmem((group * HEADS, HDIM), F32),
        vmem((oc // 128, group, 128), F32),
        vmem((slots, width), F32),
        vmem((slots, width), F32),
        vmem((slots * blocks, 128), F32),
        vmem((seqs * blocks, 128), F32),
        vmem((seqs * blocks, 128), F32),
        vmem((seqs, n_ep, 8, 128), F32),
        dma((19,)),
        dma((2,)),
        dma((2,)),
        dma((2,)),
        dma((2,)),
        dma((2,)),
        dma((2,)),
        dma((2,)),
        dma((2,)),
        pltpu.SemaphoreType.REGULAR((4,)),
    ]
    return pl.pallas_call(
        functools.partial(fused_kernel, n_ep, n_tp),
        out_shape=(
            vmem((seqs * blocks, 128), F32),
            vmem((seqs, n_tp * wkv.shape[1]), BF16),
        ),
        in_specs=[pl.BlockSpec(memory_space=pl.ANY)] * len(operands),
        out_specs=(pl.BlockSpec(memory_space=vmem), pl.BlockSpec(memory_space=vmem)),
        scratch_shapes=scratch,
        compiler_params=pltpu.CompilerParams(
            collective_id=0, has_side_effects=True, vmem_limit_bytes=66_000_000
        ),
        name="decode_layer",
    )(*operands)


def hand_over(updated, fresh, updated_out, fresh_out):
    seqs, width = updated_out.shape
    for b in range(width // 128):
        updated_out[:, b * 128 : (b + 1) * 128] = updated[
            pl.ds(b, seqs, stride=width // 128), :
        ].astype(BF16)
    fresh_out[...] = fresh[...]


def plain_copy(results, seqs):
    vmem = pl.BlockSpec(memory_space=pltpu.VMEM)
    updated, fresh = [pltpu.with_memory_space_constraint(r, pltpu.VMEM) for r in results]
    return pl.pallas_call(
        hand_over,
        out_shape=(
            jax.ShapeDtypeStruct((seqs, updated.size // seqs), BF16),
            jax.ShapeDtypeStruct(fresh.shape, BF16),
        ),
        in_specs=[vmem, vmem],
        out_specs=(vmem, vmem),
        name="hand_over",
    )(updated, fresh)


def fits(args, n_ep, n_tp):
    tokens, keys, wq, wkv, wo = args[0], args[1], args[8], args[9], args[12]
    seqs, width = tokens.shape
    return (
        n_ep in (2, 4, 8)
        and n_tp == 2 * KVH
        and n_tp * seqs == 8
        and seqs > 1
        and KVH == 2
        and wq.shape[1] % HDIM == 0
        and wq.shape[1] // HDIM < 8
        and wkv.shape[1] == HDIM
        and HDIM == 128
        and HEADS % 16 == 0
        and wo.shape[1] % 128 == 0
        and width % 2048 == 0
    )


def solution(mesh):
    in_specs = (
        P(("ep", "tp"), None),
        P(("ep", "tp"), None, None),
        P(("ep", "tp"), None, None),
        P(("ep", "tp"), None, None),
        P(("ep", "tp")),
        P(("ep", "tp"), None),
        P(("ep", "tp"), None),
        P(),
        P(None, "tp"),
        P(None, "tp"),
        P(),
        P(),
        P(None, "tp"),
        P(),
        P(),
        P("ep", None, "tp"),
        P("ep", None, "tp"),
        P("ep", "tp"),
        P("ep", "tp"),
        P("ep", "tp", None),
        P(),
    )
    out_specs = (P(("ep", "tp"), None), P(("ep", "tp"), None))
    n_ep, n_tp = mesh.shape["ep"], mesh.shape["tp"]

    def body(*args):
        if fits(args, n_ep, n_tp):
            return plain_copy(fused_device(n_ep, n_tp, *args), args[0].shape[0])
        return per_device(*args)

    return jax.shard_map(
        body, mesh=mesh, in_specs=in_specs, out_specs=out_specs, check_vma=False
    )
```

time: 36.6 us -> 28.8 us (0.79)
  Pallas kernels: 35.7 us -> 27.9 us
    pallas_call x2, Pallas kernels: 35.7 us -> 27.9 us  [the longest x1 27.3 us: fused_device(): pl.pallas_call(functools.partial(fused_kernel, n_ep, n_tp), out_shape=(vm...]
where the time goes in v1:
time: 28.8 us; the launch traced here: 28.5 us
  Pallas kernels  27.9 us (97%)
  between operations  0.65 us (2%)
    pallas_call x1, Pallas kernels, fused_device(): pl.pallas_call(functools.partial(fused_kernel, n_ep, n_tp), out_shape=(vm...  27.3 us
    pallas_call x1, Pallas kernels, plain_copy(): pl.pallas_call(hand_over, out_shape=(jax.ShapeDtypeStruct((seqs, updated....  0.61 us

profile of v1, /device:TPU:0, one launch (start us, length us, event | category | flops | bytes accessed | tf_op | source)
XLA Modules:
  0.0 28.5 jit_solution(3825876744012181203)
XLA Ops:
  0.6 27.3 %decode_layer.1 = (f32[32,128]{1,0:T(8,128)S(1)}, bf16[2,512]{1,0:T(2,128)(2,1)S(1)}) custom-call(bf16[2,2048]{1,0:T(2,128)(2,1)} %tokens.1, bf16[2,1024,256]{2,1,0:T(8,128)(2,1)} %cache_keys.1, bf16[2,1024,256]{2,1,0:T(8,128)(2,1)} %cache_values.1, f32[2,2,1024]{2,1,0:T(2,128)} %cache_gates.1, s32[1,2]{1,0:T(1,128)} %bitcast.14, s32[2,4]{1,0:T(2,128)} %routes.1, ...), custom_call_target="tpu_custom_call" | custom-call | tf_op jit(solution)/shard_map/decode_layer/pallas_call | solution.py:634
  27.9 0.6 %hand_over.1 = (bf16[2,2048]{1,0:T(2,128)(2,1)}, bf16[2,512]{1,0:T(2,128)(2,1)}) custom-call(f32[32,128]{1,0:T(8,128)S(1)} %get-tuple-element.4.updated, bf16[2,512]{1,0:T(2,128)(2,1)S(1)} %get-tuple-element.5.fresh), custom_call_target="tpu_custom_call" | custom-call | tf_op jit(solution)/shard_map/hand_over/pallas_call | solution.py:662
